TPU v7x, 256 devices: a 2x2x32 block of a 4x8x32 slice. The times are simulated.
256 devices in a mesh: grp: 4 (over y, x), ep: 64 (over z, core).
Axes of the slice: x: 2, y: 2, z: 32, core: 2. Of those that a mesh axis runs over, the one named last changes fastest.
The devices are a block of a 4x8x32 slice.
Arguments:
- tokens: bfloat16 [2048, 2048], P(('grp', 'ep')), parts along dimension 0, may hold values from -6 to 6
- first_gain: bfloat16 [2048], replicated, may hold values from 0.099609375 to 1.8984375
- query_weight: bfloat16 [2048, 1024], P(None, 'ep'), may hold values from -0.125 to 0.125
- key_weight: bfloat16 [2048, 1024], P(None, 'ep'), may hold values from -0.125 to 0.125
- value_weight: bfloat16 [2048, 1024], P(None, 'ep'), may hold values from -0.125 to 0.125
- outgate_weight: bfloat16 [2048, 1024], P(None, 'ep'), may hold values from -0.125 to 0.125
- igate_weight: bfloat16 [2048, 8], replicated, may hold values from -0.125 to 0.125
- fgate_weight: bfloat16 [2048, 8], replicated, may hold values from -0.125 to 0.125
- igate_bias: float32 [8], replicated, may hold values from -2 to 1
- fgate_bias: float32 [8], replicated, may hold values from -1 to 4
- memory_state: float32 [2048, 8, 128, 128], P(('grp', 'ep')), parts along dimension 0, may hold values from -0.6 to 0.6
- norm_state: float32 [2048, 8, 128], P(('grp', 'ep')), parts along dimension 0, may hold values from -0.6 to 0.6
- max_state: float32 [2048, 8], P(('grp', 'ep')), parts along dimension 0, may hold values from -1 to 2
- head_gain: bfloat16 [1024], replicated, may hold values from 0.099609375 to 1.8984375
- out_weight: bfloat16 [1024, 2048], P('ep'), may hold values from -0.1875 to 0.1875
- second_gain: bfloat16 [2048], replicated, may hold values from 0.099609375 to 1.8984375
- expert_ids: int32 [2048, 6], P(('grp', 'ep')), parts along dimension 0, may hold values from 0 to 63, all different within a row; in each aligned block of 8 rows (0 to 7, 8 to 15, ...) at most 2 rows name the same one
- route_weight: float32 [2048, 6], P(('grp', 'ep')), parts along dimension 0, may hold values from 0.2 to 1
- expert_gate: bfloat16 [64, 2048, 256], P('ep'), may hold values from -0.125 to 0.125
- expert_up: bfloat16 [64, 2048, 256], P('ep'), may hold values from -0.125 to 0.125
- expert_down: bfloat16 [64, 256, 2048], P('ep'), may hold values from -0.375 to 0.375
- shared_gate: bfloat16 [2048, 256], P('ep'), may hold values from -0.125 to 0.125
- shared_up: bfloat16 [2048, 256], P('ep'), may hold values from -0.125 to 0.125
- shared_down: bfloat16 [256, 2048], P(None, 'ep'), may hold values from -0.375 to 0.375
Outputs:
- mixed_out: bfloat16 [2048, 2048], P(('grp', 'ep')), parts along dimension 0
- memory_next: float32 [2048, 8, 128, 128], P(('grp', 'ep')), parts along dimension 0
- norm_next: float32 [2048, 8, 128], P(('grp', 'ep')), parts along dimension 0
- max_next: float32 [2048, 8], P(('grp', 'ep')), parts along dimension 0
There are 4 independent parts, one for each index of `grp`. A program takes and returns all parts, laid end to end along the dimension named above; an argument that names none is the same for every part. Nothing has to cross between parts.
Inputs may be any that keep to these rules, and one draw needn't show every extreme that they name: `expert_ids`: each row names 6 different experts. Among the rows of one device no expert is named by more than 2 rows, and in every draw some expert is named by exactly 2 rows of some device.
All inputs are finite; a program needn't handle non-finite values.
Results may differ from a plain program's by a relative error of at most 0.013.
Values may be sent and summed in bfloat16 or wider, within the bound.
No kernel may reach another device: no remote copies, remote signals or barrier semaphores. Data moves between devices by JAX's collectives and lax.ppermute only.
A program may use at most 64 MiB of HBM per device.

v0:
```python
import jax
import jax.numpy as jnp
from jax import lax
from jax.sharding import Mesh
from jax.sharding import PartitionSpec as P

FAR = "za"
NEAR = ("zm", "zb", "core")
ROW = ("za", "zm")
EP = ("za", "zm", "zb", "core")
GRP_EP = ("grp", "za", "zm", "zb", "core")
epsilon = 1e-06


def rms_scale(values, gain):
    return (
        values
        * lax.rsqrt(jnp.mean(values * values, axis=-1, keepdims=True) + epsilon)
        * gain.astype(jnp.float32)
    )


def cell_step(
    normed,
    query,
    key_proj,
    value_proj,
    outgate,
    igate_weight,
    fgate_weight,
    igate_bias,
    fgate_bias,
    memory_state,
    norm_state,
    max_state,
    head_gain,
):
    row_count, head_count = max_state.shape
    head_size = memory_state.shape[-1]
    input_gate = jnp.dot(normed, igate_weight, preferred_element_type=jnp.float32) + igate_bias
    forget_log = jax.nn.log_sigmoid(
        jnp.dot(normed, fgate_weight, preferred_element_type=jnp.float32) + fgate_bias
    )
    query_heads = query.astype(jnp.float32).reshape(row_count, head_count, head_size)
    key_heads = key_proj.astype(jnp.float32).reshape(
        row_count, head_count, head_size
    ) * head_size ** (-0.5)
    value_heads = value_proj.astype(jnp.float32).reshape(row_count, head_count, head_size)
    max_next = jnp.maximum(forget_log + max_state, input_gate)
    decay_rate = jnp.exp(forget_log + max_state - max_next)
    injected = jnp.exp(input_gate - max_next)
    memory_next = decay_rate[:, :, None, None] * memory_state + injected[:, :, None, None] * (
        key_heads[:, :, :, None] * value_heads[:, :, None, :]
    )
    norm_next = decay_rate[:, :, None] * norm_state + injected[:, :, None] * key_heads
    numerator = jnp.einsum(
        "shd,shde->she", query_heads, memory_next, precision=lax.Precision.HIGHEST
    )
    denominator = jnp.maximum(
        jnp.abs(jnp.sum(query_heads * norm_next, axis=-1)), jnp.exp(-max_next)
    )
    readout = numerator / denominator[:, :, None]
    readout = rms_scale(readout, head_gain.reshape(head_count, head_size))
    gated = readout.reshape(row_count, head_count * head_size) * jax.nn.sigmoid(
        outgate.astype(jnp.float32)
    )
    return (gated.astype(jnp.bfloat16), memory_next, norm_next, max_next)


def rounded(values, kind):
    info = jnp.finfo(kind)
    return lax.reduce_precision(values, info.nexp, info.nmant)


def from_peer(values, axis):
    return lax.ppermute(values, axis, [(0, 1), (1, 0)])


def in_order(values, axis_names, first):
    for place, name in enumerate(axis_names, first):
        values = jnp.where(lax.axis_index(name) == 0, values, jnp.flip(values, place))
    return values


def earlier_count(named, axis):
    count = named.shape[axis]
    before = jnp.arange(count)[:, None] < jnp.arange(count)[None, :]
    moved = jnp.moveaxis(named, axis, -1)
    counts = jnp.sum(jnp.where(before, moved[..., :, None], 0.0), axis=-2)
    return jnp.moveaxis(counts, -1, axis)


def split_two(values, kind):
    high = rounded(values, kind)
    return (high.astype(kind), (values - high).astype(kind))


def shards(
    tokens,
    first_gain,
    query_weight,
    key_weight,
    value_weight,
    outgate_weight,
    igate_weight,
    fgate_weight,
    igate_bias,
    fgate_bias,
    memory_state,
    norm_state,
    max_state,
    head_gain,
    out_weight,
    second_gain,
    expert_ids,
    route_weight,
    expert_gate,
    expert_up,
    expert_down,
    shared_gate,
    shared_up,
    shared_down,
):
    f32, bf16, f16 = (jnp.float32, jnp.bfloat16, jnp.float16)
    rows, width = tokens.shape
    top = expert_ids.shape[1]
    far = lax.axis_size(FAR)
    near = lax.axis_size(NEAR)
    row = lax.axis_size(ROW)
    devices = far * near
    members = devices // row
    slots = max(2, 2 * rows * top // devices)
    my_far = lax.axis_index(FAR)
    share = query_weight.shape[1]
    own = jnp.concatenate([query_weight.T, key_weight.T, value_weight.T, outgate_weight.T], axis=0)
    beside = from_peer(own, "zb")
    inputs = tokens.astype(f32)
    normed_exact = rounded(rms_scale(inputs, first_gain), bf16)
    normed = normed_exact.astype(bf16)
    weight_high, weight_low = split_two(route_weight, f16)
    notes = jnp.concatenate([expert_ids.astype(f16), weight_high, weight_low], axis=1)
    notes = jnp.pad(notes, ((0, 0), (0, 128 - notes.shape[1])))
    out_parts = out_weight.shape[0] // rows
    payload = jnp.concatenate(
        [normed_exact.astype(f16)]
        + [out_weight[i * rows : (i + 1) * rows].astype(f16) for i in range(out_parts)]
        + [notes],
        axis=1,
    )
    payload, beside = lax.optimization_barrier((payload, beside))
    column_weights = jnp.concatenate([own, beside], axis=0)
    other_weights = from_peer(column_weights, "core")
    gathered = lax.all_gather(payload, ROW, axis=0, tiled=True)
    block_rows = gathered[:, :width].astype(bf16)
    out_own = gathered[:, width : width * (1 + out_parts)]
    out_beside = from_peer(out_own, "zb")
    my_notes = gathered[:, width * (1 + out_parts) :].reshape(far, row // far, rows, 128)
    at_mine = lax.dynamic_index_in_dim(
        my_notes, lax.axis_index("zm"), axis=1, keepdims=False
    ).astype(f32)
    columns = jnp.concatenate(
        [
            lax.dot_general(
                block_rows, weights, (((1,), (1,)), ((), ())), preferred_element_type=f32
            )
            for weights in (column_weights, other_weights)
        ],
        axis=1,
    ).astype(bf16)
    projected = lax.all_to_all(
        columns.reshape(row, rows, columns.shape[1]), ROW, split_axis=0, concat_axis=0, tiled=True
    )
    projected, out_beside = lax.optimization_barrier((projected, out_beside))
    out_pair = jnp.stack([out_own, out_beside])
    out_other = from_peer(out_pair, "core")
    projected = projected.reshape(row, rows, 2, 2, 4, share).transpose(4, 1, 0, 3, 2, 5)
    projected = in_order(projected, ("zb", "core"), 3)
    projected = projected.reshape(4, rows, devices * share)
    slot_ids = jnp.arange(slots, dtype=f32)
    block_experts = (my_far * near).astype(f32) + jnp.arange(near, dtype=f32)
    hits = (at_mine[:, :, :top, None] == block_experts).astype(f32)
    weights = at_mine[:, :, top : 2 * top] + at_mine[:, :, 2 * top : 3 * top]
    hit = jnp.sum(hits, axis=2)
    hit_weight = jnp.sum(hits * weights[..., None], axis=2)
    hit_place = earlier_count(hit, 1)
    chosen = (hit_place[..., None] == slot_ids) * hit[..., None]
    same = (jnp.arange(far)[:, None] == jnp.arange(far))[:, None, None, :, None]
    chosen = jnp.where(same, chosen[:, :, :, None, :], 0.0)
    chosen = chosen.reshape(far * rows, near, far * slots)
    mixer = (chosen * hit_weight.reshape(far * rows, near, 1)).reshape(far * rows, -1)
    mixer_high, mixer_low = split_two(mixer, bf16)
    selector = chosen.reshape(far * rows, -1).astype(bf16)
    gated, memory_next, norm_next, max_next = cell_step(
        normed,
        projected[0],
        projected[1],
        projected[2],
        projected[3],
        igate_weight,
        fgate_weight,
        igate_bias,
        fgate_bias,
        memory_state,
        norm_state,
        max_state,
        head_gain,
    )
    spread = gated.reshape(rows, row, 2, 2, out_parts, -1).transpose(3, 2, 4, 0, 1, 5)
    spread = in_order(spread, ("core", "zb"), 0).reshape(2, 2, out_parts, rows, -1)
    mix_sums = jnp.zeros((rows, width), f32)
    for core, halves in enumerate((out_pair, out_other)):
        for zb in range(2):
            for part in range(out_parts):
                mix_sums = mix_sums + jnp.dot(
                    spread[core, zb, part],
                    halves[zb, :, part * width : (part + 1) * width].astype(bf16),
                    preferred_element_type=f32,
                )
    stream = inputs + mix_sums.astype(bf16).astype(f32)
    normed_exact = rounded(rms_scale(stream, second_gain), bf16)
    normed_two = normed_exact.astype(bf16)
    hidden = shared_gate.shape[1]
    depth = shared_gate.shape[0]
    cut = depth // rows
    piece = width // cut
    payload = jnp.concatenate(
        [
            jnp.concatenate(
                [normed_exact[:, i * piece : (i + 1) * piece] for i in range(cut)], axis=0
            ).astype(f16),
            shared_gate.astype(f16),
            shared_up.astype(f16),
            shared_down.T.astype(f16),
        ],
        axis=1,
    )
    gathered = lax.all_gather(payload, FAR, axis=0, tiled=True)
    far_rows = gathered[:, :piece].reshape(far, cut, rows, piece).transpose(0, 2, 1, 3)
    far_rows = far_rows.reshape(far * rows, width).astype(bf16)
    shared_one = gathered[:, piece:]
    shared_beside = from_peer(shared_one, "zm")
    outgoing = lax.dot_general(
        selector, far_rows, (((0,), (0,)), ((), ())), preferred_element_type=f32
    ).astype(bf16)
    flat_rows = lax.all_to_all(
        outgoing.reshape(near, far * slots, width), NEAR, split_axis=0, concat_axis=0, tiled=True
    ).reshape(near * far * slots, width)
    flat_rows, shared_beside = lax.optimization_barrier((flat_rows, shared_beside))
    shared_two = jnp.stack([shared_one, shared_beside])
    shared_beside = from_peer(shared_two, "zb")
    gate_sums = jnp.dot(flat_rows, expert_gate[0], preferred_element_type=f32)
    up_sums = jnp.dot(flat_rows, expert_up[0], preferred_element_type=f32)
    hidden_rows = (jax.nn.silu(gate_sums) * up_sums).astype(bf16)
    result = jnp.dot(hidden_rows, expert_down[0], preferred_element_type=f32).astype(bf16)
    near_results = lax.all_to_all(
        result.reshape(near, far * slots, width), NEAR, split_axis=0, concat_axis=0, tiled=True
    ).reshape(near * far * slots, width)
    near_results, shared_beside = lax.optimization_barrier((near_results, shared_beside))
    shared_four = jnp.stack([shared_two, shared_beside])
    shared_other = from_peer(shared_four, "core")
    partial = jnp.dot(mixer_high, near_results, preferred_element_type=f32) + jnp.dot(
        mixer_low, near_results, preferred_element_type=f32
    )
    far_sums = lax.all_to_all(
        partial.astype(bf16).reshape(far, rows, width), FAR, split_axis=0, concat_axis=0, tiled=True
    )
    routed = jnp.sum(far_sums.astype(f32), axis=0)
    by_member = normed_two.reshape(rows, far, 2, 2, 2, depth).transpose(4, 3, 2, 0, 1, 5)
    by_member = in_order(by_member, ("core", "zb", "zm"), 0).reshape(near, rows, far * depth)
    shared_all = jnp.concatenate(
        [
            shared_four.reshape(near // 2, far * depth, -1),
            shared_other.reshape(near // 2, far * depth, -1),
        ]
    ).astype(bf16)
    gate_up = lax.dot_general(
        by_member,
        shared_all[:, :, : 2 * hidden],
        (((2,), (1,)), ((0,), (0,))),
        preferred_element_type=f32,
    )
    gate_up = jnp.sum(gate_up, axis=0)
    hidden_shared = (jax.nn.silu(gate_up[:, :hidden]) * gate_up[:, hidden:]).astype(bf16)
    shared_result = lax.dot_general(
        hidden_shared,
        shared_all[:, :, 2 * hidden :],
        (((1,), (2,)), ((), ())),
        preferred_element_type=f32,
    )
    shared_result = shared_result.reshape(rows, 2, 2, 2, far, depth).transpose(0, 4, 3, 2, 1, 5)
    shared_result = in_order(shared_result, NEAR, 2).reshape(rows, width)
    mixed_out = (stream + routed + shared_result).astype(bf16)
    return (mixed_out, memory_next, norm_next, max_next)


def solution(mesh):
    torus = Mesh(mesh.devices.reshape(mesh.shape["grp"], 8, 2, 2, 2), GRP_EP)
    placed = (
        P(GRP_EP, None),
        P(),
        P(None, EP),
        P(None, EP),
        P(None, EP),
        P(None, EP),
        P(),
        P(),
        P(),
        P(),
        P(GRP_EP, None, None, None),
        P(GRP_EP, None, None),
        P(GRP_EP, None),
        P(),
        P(EP, None),
        P(),
        P(GRP_EP, None),
        P(GRP_EP, None),
        P(EP, None, None),
        P(EP, None, None),
        P(EP, None, None),
        P(EP, None),
        P(EP, None),
        P(None, EP),
    )
    return jax.shard_map(
        shards,
        mesh=torus,
        in_specs=placed,
        out_specs=(
            P(GRP_EP, None),
            P(GRP_EP, None, None, None),
            P(GRP_EP, None, None),
            P(GRP_EP, None),
        ),
        check_vma=False,
    )
```

profile of v0, /device:TPU:102, one launch (start us, length us, event | category | flops | bytes accessed | tf_op | source)
XLA Modules:
  0.0 358.0 jit_solution(3707160827783618954)
XLA Ops:
  1.9 1.5 constant_dynamic-update-slice_fusion.4
  9.4 1.6 broadcast_multiply_fusion.1
  13.0 1.5 constant_dynamic-update-slice_fusion.3
  14.5 1.5 constant_dynamic-update-slice_fusion.2
  15.9 1.5 constant_dynamic-update-slice_fusion.1
  22.8 79.3 %all-gather.1 = f16[128,6272]{1,0:T(8,128)(2,1)S(1)} all-gather(f16[8,6272]{1,0:T(8,128)(2,1)S(1)} %pad_maximum_fusion.4), channel_id=1, replica_groups=mesh['grp'=4,'za'=8,'zm'=2,'zb'=2,'core'=2] {'za','zm'}, dimensions={0}, use_global_device_ids=true | all-gather | bytes 1705984 | tf_op jit(solution)/shard_map/all_gather | solution.py:153
  106.5 1.5 fusion.10
  108.0 1.5 fusion.11
  110.2 8.9 %all-to-all-start = ((bf16[16,8,256]{2,1,0:T(8,128)(2,1)}), bf16[16,8,256]{2,1,0:T(8,128)(2,1)S(1)}, u32[]{:S(2)}, u32[]{:S(2)}) async-start(bf16[16,8,256]{2,1,0:T(8,128)(2,1)} %pad_maximum_fusion.6), calls=%async_computation | async-start | bytes 131072 | tf_op jit(solution)/shard_map/all_to_all | solution.py:170
  120.2 23.3 %all-to-all-done = bf16[16,8,256]{2,1,0:T(8,128)(2,1)S(1)} async-done(((bf16[16,8,256]{2,1,0:T(8,128)(2,1)}), bf16[16,8,256]{2,1,0:T(8,128)(2,1)S(1)}, u32[]{:S(2)}, u32[]{:S(2)}) %all-to-all-start) | async-done | bytes 65568 | tf_op jit(solution)/shard_map/all_to_all | solution.py:170
  149.5 1.8 copy.62
  151.3 1.9 reshape.215
  153.2 1.5 multiply_reduce_fusion.2
  155.4 1.8 copy.63
  157.1 1.9 reshape.216
  160.1 1.8 pad_maximum_fusion
  163.0 2.6 multiply_add_fusion
  165.6 2.0 fusion.82
  167.9 1.6 reshape.201
  169.5 1.5 fusion.46
  177.9 45.1 %all_gather.7 = f16[256,1280]{1,0:T(8,128)(2,1)S(1)} all-gather(f16[32,1280]{1,0:T(8,128)(2,1)S(1)} %pad_maximum_fusion.5), channel_id=1, replica_groups=mesh['grp'=4,'za'=8,'zm'=2,'zb'=2,'core'=2] {'za'}, dimensions={0}, use_global_device_ids=true | all-gather | bytes 737280 | tf_op jit(solution)/shard_map/all_gather | solution.py:237
  224.1 3.6 all-to-all-start.1
  227.8 2.2 collective-permute-start.4
  230.0 26.1 %collective-permute-done.4 = f16[256,768]{1,0:T(8,128)(2,1)S(1)} collective-permute-done((f16[256,768]{1,0:T(8,128)(2,1)S(1)}, f16[256,768]{1,0:T(8,128)(2,1)S(1)}, u32[]{:S(2)}, u32[]{:S(2)}) %collective-permute-start.4) | collective-permute-done | bytes 393248 | tf_op jit(solution)/shard_map/ppermute | solution.py:76
  256.1 1.5 fusion.22
  257.6 2.8 convolution_convert_fusion
  260.5 7.0 %all-to-all-start.2 = ((bf16[8,16,2048]{2,1,0:T(8,128)(2,1)}), bf16[8,16,2048]{2,1,0:T(8,128)(2,1)S(1)}, u32[]{:S(2)}, u32[]{:S(2)}) async-start(bf16[8,16,2048]{2,1,0:T(8,128)(2,1)} %bitcast.47), calls=%async_computation.2 | async-start | bytes 1048576 | tf_op jit(solution)/shard_map/all_to_all | solution.py:255
  268.8 25.5 %collective-permute-done.5 = f16[2,256,768]{2,1,0:T(8,128)(2,1)S(1)} collective-permute-done((f16[2,256,768]{2,1,0:T(8,128)(2,1)S(1)}, f16[2,256,768]{2,1,0:T(8,128)(2,1)S(1)}, u32[]{:S(2)}, u32[]{:S(2)}) %collective-permute-start.5) | collective-permute-done | bytes 786464 | tf_op jit(solution)/shard_map/ppermute | solution.py:76
  295.2 1.7 pad_maximum_fusion.1
  301.6 14.4 %all-to-all-start.3 = ((bf16[8,8,2048]{2,1,0:T(8,128)(2,1)}), bf16[8,8,2048]{2,1,0:T(8,128)(2,1)S(1)}, u32[]{:S(2)}, u32[]{:S(2)}) async-start(bf16[8,8,2048]{2,1,0:T(8,128)(2,1)} %fusion.1), calls=%async_computation.3 | async-start | bytes 524288 | tf_op jit(solution)/shard_map/all_to_all | solution.py:264
  316.6 1.9 maximum_convert_fusion
  322.2 35.1 %all-to-all-done.3 = bf16[8,8,2048]{2,1,0:T(8,128)(2,1)S(1)} async-done(((bf16[8,8,2048]{2,1,0:T(8,128)(2,1)}), bf16[8,8,2048]{2,1,0:T(8,128)(2,1)S(1)}, u32[]{:S(2)}, u32[]{:S(2)}) %all-to-all-start.3) | async-done | bytes 262176 | tf_op jit(solution)/shard_map/all_to_all | solution.py:264
  (146 shorter events, 49.6 us)
Async XLA Ops:
  0.6 257.0 %copy-start = (bf16[1,256,2048]{2,1,0:T(8,128)(2,1)S(1)}, bf16[1,256,2048]{2,1,0:T(8,128)(2,1)}, u32[]{:S(2)}) copy-start(bf16[1,256,2048]{2,1,0:T(8,128)(2,1)} %param.44) | copy-start | bytes 3145732
  1.7 21.1 %collective-permute-start = (bf16[64,2048]{1,0:T(8,128)(2,1)S(1)}, bf16[64,2048]{1,0:T(8,128)(2,1)S(1)}, u32[]{:S(2)}, u32[]{:S(2)}) collective-permute-start(bf16[64,2048]{1,0:T(8,128)(2,1)S(1)} %pad_maximum_fusion.3), channel_id=1, source_target_pairs={{0,2},{2,0},{1,3},{3,1},{4,6},{6,4},{5,7},{7,5},{8,10},{10,8},{9,1... | collective-permute-start | bytes 786440 | tf_op jit(solution)/shard_map/ppermute | solution.py:76
  1.9 117.5 %copy-start.16 = (pred[8,8]{0,1:T(8,128)(4,1)}, pred[8,8]{0,1:T(8,128)(4,1)S(1)}, u32[]{:S(2)}) copy-start(pred[8,8]{0,1:T(8,128)(4,1)S(1)} %iota_compare_fusion.3) | copy-start | bytes 196
  11.0 0.6 copy-start.13
  102.0 1.2 copy-start.2
  105.2 2.8 collective-permute-start.1
  105.5 38.1 %collective-permute-start.2 = (f16[128,4096]{1,0:T(8,128)(2,1)}, f16[128,4096]{1,0:T(8,128)(2,1)S(1)}, u32[]{:S(2)}, u32[]{:S(2)}) collective-permute-start(f16[128,4096]{1,0:T(8,128)(2,1)} %get-tuple-element.28), channel_id=1, source_target_pairs={{0,2},{2,0},{1,3},{3,1},{4,6},{6,4},{5,7},{7,5},{8,10},{10,8},{9,1... | collective-permute-start | bytes 3145736 | tf_op jit(solution)/shard_map/ppermute | solution.py:76
  110.2 33.4 %all-to-all-start = ((bf16[16,8,256]{2,1,0:T(8,128)(2,1)}), bf16[16,8,256]{2,1,0:T(8,128)(2,1)S(1)}, u32[]{:S(2)}, u32[]{:S(2)}) async-start(bf16[16,8,256]{2,1,0:T(8,128)(2,1)} %pad_maximum_fusion.6), calls=%async_computation | async-start | bytes 131072 | tf_op jit(solution)/shard_map/all_to_all | solution.py:170
  159.0 2.9 copy-start.11
  159.0 2.9 copy-start.15
  160.1 2.9 copy-start.3
  161.9 10.8 %collective-permute-start.3 = (f16[2,128,4096]{2,1,0:T(8,128)(2,1)}, f16[2,128,4096]{2,1,0:T(8,128)(2,1)}, u32[]{:S(2)}, u32[]{:S(2)}) collective-permute-start(f16[2,128,4096]{2,1,0:T(8,128)(2,1)} %pad_maximum_fusion), channel_id=1, source_target_pairs={{0,1},{1,0},{2,3},{3,2},{4,5},{5,4},{6,7},{7,6},{8,9},{9,8},{10,11... | collective-permute-start | bytes 6291464 | tf_op jit(solution)/shard_map/ppermute | solution.py:76
  165.6 2.0 copy-start.1
  165.6 2.2 copy-start.14
  171.9 4.5 %copy-start.5 = (bf16[8,2048]{1,0:T(8,128)(2,1)S(1)}, bf16[8,2048]{1,0:T(8,128)(2,1)}, u32[]{:S(2)}) copy-start(bf16[8,2048]{1,0:T(8,128)(2,1)} %param.24) | copy-start | bytes 98308
  172.2 5.4 %copy-start.12 = (f32[2048]{0:T(1024)S(1)}, f32[2048]{0:T(1024)}, u32[]{:S(2)}) copy-start(f32[2048]{0:T(1024)} %convert_element_type.262) | copy-start | bytes 24580
  172.2 5.6 %copy-start.8 = (f16[32,256]{1,0:T(8,128)(2,1)S(1)}, f16[32,256]{1,0:T(8,128)(2,1)}, u32[]{:S(2)}) copy-start(f16[32,256]{1,0:T(8,128)(2,1)} %convert_element_type.263) | copy-start | bytes 49156
  172.2 5.6 %copy-start.9 = (f16[32,256]{1,0:T(8,128)(2,1)S(1)}, f16[32,256]{1,0:T(8,128)(2,1)}, u32[]{:S(2)}) copy-start(f16[32,256]{1,0:T(8,128)(2,1)} %convert_element_type.264) | copy-start | bytes 49156
  172.3 5.6 %copy-start.10 = (f16[32,256]{1,0:T(8,128)(2,1)S(1)}, f16[32,256]{1,0:T(8,128)(2,1)}, u32[]{:S(2)}) copy-start(f16[32,256]{1,0:T(8,128)(2,1)} %convert_bitcast_fusion) | copy-start | bytes 49156
  172.6 50.4 %copy-start.6 = (bf16[64,128]{0,1:T(8,128)(2,1)S(1)}, bf16[64,128]{0,1:T(8,128)(2,1)}, u32[]{:S(2)}) copy-start(bf16[64,128]{0,1:T(8,128)(2,1)} %convert_element_type.261) | copy-start | bytes 49156
  224.1 32.0 %all-to-all-start.1 = ((bf16[8,16,2048]{2,1,0:T(8,128)(2,1)}), bf16[8,16,2048]{2,1,0:T(8,128)(2,1)S(1)}, u32[]{:S(2)}, u32[]{:S(2)}) async-start(bf16[8,16,2048]{2,1,0:T(8,128)(2,1)} %bitcast.42), calls=%async_computation.1 | async-start | bytes 1048576 | tf_op jit(solution)/shard_map/all_to_all | solution.py:245
  227.8 28.3 %collective-permute-start.4 = (f16[256,768]{1,0:T(8,128)(2,1)S(1)}, f16[256,768]{1,0:T(8,128)(2,1)S(1)}, u32[]{:S(2)}, u32[]{:S(2)}) collective-permute-start(f16[256,768]{1,0:T(8,128)(2,1)S(1)} %get-tuple-element.32), channel_id=1, source_target_pairs={{0,4},{4,0},{1,5},{5,1},{2,6},{6,2},{3,7},{7,3},{8,12},{12,8},{9,1... | collective-permute-start | bytes 1179656 | tf_op jit(solution)/shard_map/ppermute | solution.py:76
  260.5 33.8 %all-to-all-start.2 = ((bf16[8,16,2048]{2,1,0:T(8,128)(2,1)}), bf16[8,16,2048]{2,1,0:T(8,128)(2,1)S(1)}, u32[]{:S(2)}, u32[]{:S(2)}) async-start(bf16[8,16,2048]{2,1,0:T(8,128)(2,1)} %bitcast.47), calls=%async_computation.2 | async-start | bytes 1048576 | tf_op jit(solution)/shard_map/all_to_all | solution.py:255
  268.5 28.6 %copy-start.17 = (pred[8,8]{0,1:T(8,128)(4,1)S(1)}, pred[8,8]{0,1:T(8,128)(4,1)}, u32[]{:S(2)}) copy-start(pred[8,8]{0,1:T(8,128)(4,1)} %copy-done.16) | copy-start | bytes 196
  268.5 28.8 %copy-start.7 = (f32[8,8,8]{2,1,0:T(8,128)S(1)}, f32[8,8,8]{2,1,0:T(8,128)}, u32[]{:S(2)}) copy-start(f32[8,8,8]{2,1,0:T(8,128)} %get-tuple-element.20) | copy-start | bytes 6148
  268.5 25.8 %collective-permute-start.5 = (f16[2,256,768]{2,1,0:T(8,128)(2,1)S(1)}, f16[2,256,768]{2,1,0:T(8,128)(2,1)S(1)}, u32[]{:S(2)}, u32[]{:S(2)}) collective-permute-start(f16[2,256,768]{2,1,0:T(8,128)(2,1)S(1)} %get-tuple-element.30), channel_id=1, source_target_pairs={{0,2},{2,0},{1,3},{3,1},{4,6},{6,4},{5,7},{7,5},{8,10},{10,8},{9,1... | collective-permute-start | bytes 2359304 | tf_op jit(solution)/shard_map/ppermute | solution.py:76
  294.3 0.9 copy-start.4
  297.0 19.7 %collective-permute-start.6 = (f16[2,2,256,768]{3,2,1,0:T(8,128)(2,1)S(1)}, f16[2,2,256,768]{3,2,1,0:T(8,128)(2,1)}, u32[]{:S(2)}, u32[]{:S(2)}) collective-permute-start(f16[2,2,256,768]{3,2,1,0:T(8,128)(2,1)S(1)} %pad_maximum_fusion.1), channel_id=1, source_target_pairs={{0,1},{1,0},{2,3},{3,2},{4,5},{5,4},{6,7},{7,6},{8,9},{9,8},{10,11... | collective-permute-start | bytes 4718600 | tf_op jit(solution)/shard_map/ppermute | solution.py:76
  301.6 55.7 %all-to-all-start.3 = ((bf16[8,8,2048]{2,1,0:T(8,128)(2,1)}), bf16[8,8,2048]{2,1,0:T(8,128)(2,1)S(1)}, u32[]{:S(2)}, u32[]{:S(2)}) async-start(bf16[8,8,2048]{2,1,0:T(8,128)(2,1)} %fusion.1), calls=%async_computation.3 | async-start | bytes 524288 | tf_op jit(solution)/shard_map/all_to_all | solution.py:264
where the time goes:
time: 360 us; the launch traced here: 358 us
  blocking collectives  124 us (34%)
  waiting for transfers between devices  110 us (31%)
  starting transfers between devices  36.7 us (10%)
  local copies, waits for them, and re-layouts  31.9 us (9%)
  other arithmetic  31.9 us (9%)
  matrix products  21.8 us (6%)
    all_gather x1, blocking collectives, shards(): gathered = lax.all_gather(payload, ROW, axis=0, tiled=True)  79.3 us
    ppermute x7, waiting for transfers between devices, from_peer(): return lax.ppermute(values, axis, [(0, 1), (1, 0)])  51.6 us
    all_gather x1, blocking collectives, shards(): gathered = lax.all_gather(payload, FAR, axis=0, tiled=True)  45.1 us
    all_to_all x1, waiting for transfers between devices, shards(): lax.all_to_all(partial.astype(bf16).reshape(far, rows, width), FAR, split...  35.1 us
    all_to_all x1, waiting for transfers between devices, shards(): lax.all_to_all(columns.reshape(row, rows, columns.shape[1]), ROW, split_a...  23.3 us
    all_to_all x1, starting transfers between devices, shards(): lax.all_to_all(partial.astype(bf16).reshape(far, rows, width), FAR, split...  14.4 us
    unnamed x40, local copies, waits for them, and re-layouts  9.69 us
    all_to_all x1, starting transfers between devices, shards(): lax.all_to_all(columns.reshape(row, rows, columns.shape[1]), ROW, split_a...  8.88 us
  transfers between devices with their start and end apart: 11, of which 4 were waited for; matrix products, arithmetic and copies ran while one was open for 13% of the time, Pallas kernels for 0%

commit v1 on v0

--- a/solution.py
+++ b/solution.py
@@ -234,7 +234,9 @@
         ],
         axis=1,
     )
-    gathered = lax.all_gather(payload, FAR, axis=0, tiled=True)
+    gathered = jnp.concatenate(
+        lax.all_to_all(jnp.stack([payload] * lax.axis_size(FAR)), FAR, 0, 0), axis=0
+    )
     far_rows = gathered[:, :piece].reshape(far, cut, rows, piece).transpose(0, 2, 1, 3)
     far_rows = far_rows.reshape(far * rows, width).astype(bf16)
     shared_one = gathered[:, piece:]

time: 360 us -> 373 us (1.036)
  waiting for transfers between devices: 110 us -> 175 us
  blocking collectives: 124 us -> 74.4 us
  starting transfers between devices: 36.7 us -> 48.6 us
  other arithmetic: 31.9 us -> 25.6 us
  local copies, waits for them, and re-layouts: 31.9 us -> 26.3 us
    all_to_all x0 -> x1, waiting for transfers between devices: none -> 69.2 us  [shards(): lax.all_to_all(jnp.stack([payload] * lax.axis_size(FAR)), FAR, 0, 0)]
    all_gather x1 -> x0, blocking collectives: 45.1 us -> none  [shards(): gathered = lax.all_gather(payload, FAR, axis=0, tiled=True)]
    all_to_all x1, starting transfers between devices: 14.4 us -> 3.84 us  [shards(): lax.all_to_all(partial.astype(bf16).reshape(far, rows, width), FAR, split...]
    all_to_all x1, starting transfers between devices: 8.88 us -> 17 us  [shards(): lax.all_to_all(columns.reshape(row, rows, columns.shape[1]), ROW, split_a...]
    all_to_all x1, starting transfers between devices: 3.57 us -> 8.97 us  [shards(): lax.all_to_all(outgoing.reshape(near, far * slots, width), NEAR, split_ax...]
    ppermute x7, starting transfers between devices: 2.91 us -> 7.86 us  [from_peer(): return lax.ppermute(values, axis, [(0, 1), (1, 0)])]
    all_gather x1, blocking collectives: 79.3 us -> 74.4 us  [shards(): gathered = lax.all_gather(payload, ROW, axis=0, tiled=True)]
    unnamed x40 -> x38, local copies, waits for them, and re-layouts: 9.69 us -> 5.52 us
  transfers between devices with their start and end apart: 11 -> 12, of which waited for: 4 -> 5; matrix products, arithmetic and copies ran while one was open for 13% -> 10% of each run, Pallas kernels for 0% -> 0%
where the time goes in v1:
time: 373 us; the launch traced here: 371 us
  waiting for transfers between devices  175 us (47%)
  blocking collectives  74.4 us (20%)
  starting transfers between devices  48.6 us (13%)
  local copies, waits for them, and re-layouts  26.3 us (7%)
  other arithmetic  25.6 us (7%)
  matrix products  19.4 us (5%)
    all_gather x1, blocking collectives, shards(): gathered = lax.all_gather(payload, ROW, axis=0, tiled=True)  74.4 us
    all_to_all x1, waiting for transfers between devices, shards(): lax.all_to_all(jnp.stack([payload] * lax.axis_size(FAR)), FAR, 0, 0)  69.2 us
    ppermute x7, waiting for transfers between devices, from_peer(): return lax.ppermute(values, axis, [(0, 1), (1, 0)])  51.6 us
    all_to_all x1, waiting for transfers between devices, shards(): lax.all_to_all(partial.astype(bf16).reshape(far, rows, width), FAR, split...  35 us
    all_to_all x1, waiting for transfers between devices, shards(): lax.all_to_all(columns.reshape(row, rows, columns.shape[1]), ROW, split_a...  19.4 us
    all_to_all x1, starting transfers between devices, shards(): lax.all_to_all(columns.reshape(row, rows, columns.shape[1]), ROW, split_a...  17 us
    all_to_all x1, starting transfers between devices, shards(): lax.all_to_all(outgoing.reshape(near, far * slots, width), NEAR, split_ax...  8.97 us
    ppermute x7, starting transfers between devices, from_peer(): return lax.ppermute(values, axis, [(0, 1), (1, 0)])  7.86 us
  transfers between devices with their start and end apart: 12, of which 5 were waited for; matrix products, arithmetic and copies ran while one was open for 10% of the time, Pallas kernels for 0%

profile of v1, /device:TPU:102, one launch (start us, length us, event | category | flops | bytes accessed | tf_op | source)
XLA Modules:
  0.0 370.7 jit_solution(16074158664609318631)
XLA Ops:
  10.9 1.6 broadcast_multiply_fusion.1
  12.7 74.4 %all-gather.1 = f16[128,6272]{1,0:T(8,128)(2,1)S(1)} all-gather(f16[8,6272]{1,0:T(8,128)(2,1)S(1)} %pad_maximum_fusion.4), channel_id=1, replica_groups=mesh['grp'=4,'za'=8,'zm'=2,'zb'=2,'core'=2] {'za','zm'}, dimensions={0}, use_global_device_ids=true | all-gather | bytes 1705984 | tf_op jit(solution)/shard_map/all_gather | solution.py:153
  87.1 1.5 slice_bitcast_fusion.17
  88.6 4.7 %collective-permute-start.2 = (f16[128,4096]{1,0:T(8,128)(2,1)}, f16[128,4096]{1,0:T(8,128)(2,1)S(1)}, u32[]{:S(2)}, u32[]{:S(2)}) collective-permute-start(f16[128,4096]{1,0:T(8,128)(2,1)} %get-tuple-element.28), channel_id=1, source_target_pairs={{0,2},{2,0},{1,3},{3,1},{4,6},{6,4},{5,7},{7,5},{8,10},{10,8},{9,1... | collective-permute-start | bytes 3145736 | tf_op jit(solution)/shard_map/ppermute | solution.py:76
  94.5 17.0 %all-to-all-start = ((bf16[16,8,256]{2,1,0:T(8,128)(2,1)}), bf16[16,8,256]{2,1,0:T(8,128)(2,1)S(1)}, u32[]{:S(2)}, u32[]{:S(2)}) async-start(bf16[16,8,256]{2,1,0:T(8,128)(2,1)} %pad_maximum_fusion.6), calls=%async_computation | async-start | bytes 131072 | tf_op jit(solution)/shard_map/all_to_all | solution.py:170
  114.0 19.4 %all-to-all-done = bf16[16,8,256]{2,1,0:T(8,128)(2,1)S(1)} async-done(((bf16[16,8,256]{2,1,0:T(8,128)(2,1)}), bf16[16,8,256]{2,1,0:T(8,128)(2,1)S(1)}, u32[]{:S(2)}, u32[]{:S(2)}) %all-to-all-start) | async-done | bytes 65568 | tf_op jit(solution)/shard_map/all_to_all | solution.py:170
  134.6 1.4 copy.79
  139.4 1.8 copy.62
  141.2 1.3 reshape.221
  142.4 1.5 multiply_reduce_fusion.2
  144.6 1.8 copy.63
  146.4 1.3 reshape.222
  148.7 1.8 pad_maximum_fusion
  151.6 1.6 multiply_add_fusion
  153.2 2.0 fusion.82
  155.5 1.6 reshape.206
  157.1 1.5 fusion.46
  163.9 1.3 multiply_reduce_fusion
  166.4 4.0 %all-to-all-start.1 = ((f16[8,32,1280]{2,1,0:T(8,128)(2,1)}), f16[8,32,1280]{2,1,0:T(8,128)(2,1)S(1)}, u32[]{:S(2)}, u32[]{:S(2)}) async-start(f16[8,32,1280]{2,1,0:T(8,128)(2,1)} %stack.41), calls=%async_computation.1 | async-start | bytes 1310720 | tf_op jit(solution)/shard_map/all_to_all | solution.py:238
  171.6 69.2 %all-to-all-done.1 = f16[8,32,1280]{2,1,0:T(8,128)(2,1)S(1)} async-done(((f16[8,32,1280]{2,1,0:T(8,128)(2,1)}), f16[8,32,1280]{2,1,0:T(8,128)(2,1)S(1)}, u32[]{:S(2)}, u32[]{:S(2)}) %all-to-all-start.1) | async-done | bytes 655392 | tf_op jit(solution)/shard_map/all_to_all | solution.py:238
  241.8 9.0 %all-to-all-start.2 = ((bf16[8,16,2048]{2,1,0:T(8,128)(2,1)}), bf16[8,16,2048]{2,1,0:T(8,128)(2,1)S(1)}, u32[]{:S(2)}, u32[]{:S(2)}) async-start(bf16[8,16,2048]{2,1,0:T(8,128)(2,1)} %bitcast.43), calls=%async_computation.2 | async-start | bytes 1048576 | tf_op jit(solution)/shard_map/all_to_all | solution.py:247
  250.9 2.5 collective-permute-start.4
  253.4 26.1 %collective-permute-done.4 = f16[256,768]{1,0:T(8,128)(2,1)S(1)} collective-permute-done((f16[256,768]{1,0:T(8,128)(2,1)S(1)}, f16[256,768]{1,0:T(8,128)(2,1)S(1)}, u32[]{:S(2)}, u32[]{:S(2)}) %collective-permute-start.4) | collective-permute-done | bytes 393248 | tf_op jit(solution)/shard_map/ppermute | solution.py:76
  279.5 1.5 fusion.22
  281.0 2.8 convolution_convert_fusion
  283.8 6.9 %all-to-all-start.3 = ((bf16[8,16,2048]{2,1,0:T(8,128)(2,1)}), bf16[8,16,2048]{2,1,0:T(8,128)(2,1)S(1)}, u32[]{:S(2)}, u32[]{:S(2)}) async-start(bf16[8,16,2048]{2,1,0:T(8,128)(2,1)} %bitcast.48), calls=%async_computation.3 | async-start | bytes 1048576 | tf_op jit(solution)/shard_map/all_to_all | solution.py:257
  292.1 25.5 %collective-permute-done.5 = f16[2,256,768]{2,1,0:T(8,128)(2,1)S(1)} collective-permute-done((f16[2,256,768]{2,1,0:T(8,128)(2,1)S(1)}, f16[2,256,768]{2,1,0:T(8,128)(2,1)S(1)}, u32[]{:S(2)}, u32[]{:S(2)}) %collective-permute-start.5) | collective-permute-done | bytes 786464 | tf_op jit(solution)/shard_map/ppermute | solution.py:76
  318.6 1.7 pad_maximum_fusion.1
  324.9 3.8 %all-to-all-start.4 = ((bf16[8,8,2048]{2,1,0:T(8,128)(2,1)}), bf16[8,8,2048]{2,1,0:T(8,128)(2,1)S(1)}, u32[]{:S(2)}, u32[]{:S(2)}) async-start(bf16[8,8,2048]{2,1,0:T(8,128)(2,1)} %fusion.1), calls=%async_computation.4 | async-start | bytes 524288 | tf_op jit(solution)/shard_map/all_to_all | solution.py:266
  329.4 1.9 maximum_convert_fusion
  331.8 1.4 fusion.16
  335.0 35.0 %all-to-all-done.4 = bf16[8,8,2048]{2,1,0:T(8,128)(2,1)S(1)} async-done(((bf16[8,8,2048]{2,1,0:T(8,128)(2,1)}), bf16[8,8,2048]{2,1,0:T(8,128)(2,1)S(1)}, u32[]{:S(2)}, u32[]{:S(2)}) %all-to-all-start.4) | async-done | bytes 262176 | tf_op jit(solution)/shard_map/all_to_all | solution.py:266
  (147 shorter events, 40.8 us)
Async XLA Ops:
  0.6 280.4 %copy-start = (bf16[1,256,2048]{2,1,0:T(8,128)(2,1)S(1)}, bf16[1,256,2048]{2,1,0:T(8,128)(2,1)}, u32[]{:S(2)}) copy-start(bf16[1,256,2048]{2,1,0:T(8,128)(2,1)} %param.44) | copy-start | bytes 3145732
  1.7 10.9 %collective-permute-start = (bf16[64,2048]{1,0:T(8,128)(2,1)S(1)}, bf16[64,2048]{1,0:T(8,128)(2,1)S(1)}, u32[]{:S(2)}, u32[]{:S(2)}) collective-permute-start(bf16[64,2048]{1,0:T(8,128)(2,1)S(1)} %pad_maximum_fusion.3), channel_id=1, source_target_pairs={{0,2},{2,0},{1,3},{3,1},{4,6},{6,4},{5,7},{7,5},{8,10},{10,8},{9,1... | collective-permute-start | bytes 786440 | tf_op jit(solution)/shard_map/ppermute | solution.py:76
  12.5 100.3 %copy-start.9 = (f32[8,8]{1,0:T(8,128)}, f32[8,8]{1,0:T(8,128)S(1)}, u32[]{:S(2)}) copy-start(f32[8,8]{1,0:T(8,128)S(1)} %get-tuple-element.26) | copy-start | bytes 772
  12.6 81.0 %collective-permute-start.1 = (bf16[128,2048]{1,0:T(8,128)(2,1)S(1)}, bf16[128,2048]{1,0:T(8,128)(2,1)S(1)}, u32[]{:S(2)}, u32[]{:S(2)}) collective-permute-start(bf16[128,2048]{1,0:T(8,128)(2,1)S(1)} %constant_dynamic-update-slice_fusion), channel_id=1, source_target_pairs={{0,1},{1,0},{2,3},{3,2},{4,5},{5,4},{6,7},{7,6},{8,9},{9,8},{10,11... | collective-permute-start | bytes 1572872 | tf_op jit(solution)/shard_map/ppermute | solution.py:76
  87.1 6.5 %copy-start.2 = (f16[128,6272]{1,0:T(8,128)(2,1)}, f16[128,6272]{1,0:T(8,128)(2,1)S(1)}, u32[]{:S(2)}) copy-start(f16[128,6272]{1,0:T(8,128)(2,1)S(1)} %all-gather.1) | copy-start | bytes 4816900
  87.1 24.5 %copy-start.16 = (bf16[1024]{0:T(1024)(128)(2,1)S(1)}, bf16[1024]{0:T(1024)(128)(2,1)}, u32[]{:S(2)}) copy-start(bf16[1024]{0:T(1024)(128)(2,1)} %param.37) | copy-start | bytes 6148
  87.1 25.1 %copy-start.15 = (bf16[2048]{0:T(1024)(128)(2,1)S(1)}, bf16[2048]{0:T(1024)(128)(2,1)}, u32[]{:S(2)}) copy-start(bf16[2048]{0:T(1024)(128)(2,1)} %param.39) | copy-start | bytes 12292
  87.1 25.7 %copy-start.11 = (bf16[32,256]{1,0:T(8,128)(2,1)S(1)}, bf16[32,256]{1,0:T(8,128)(2,1)}, u32[]{:S(2)}) copy-start(bf16[32,256]{1,0:T(8,128)(2,1)} %param.45) | copy-start | bytes 49156
  87.1 25.7 %copy-start.12 = (bf16[32,256]{1,0:T(8,128)(2,1)S(1)}, bf16[32,256]{1,0:T(8,128)(2,1)}, u32[]{:S(2)}) copy-start(bf16[32,256]{1,0:T(8,128)(2,1)} %param.46) | copy-start | bytes 49156
  87.1 26.3 %copy-start.13 = (bf16[256,32]{0,1:T(8,128)(2,1)S(1)}, bf16[256,32]{0,1:T(8,128)(2,1)}, u32[]{:S(2)}) copy-start(bf16[256,32]{0,1:T(8,128)(2,1)} %param.47) | copy-start | bytes 49156
  88.6 44.8 %collective-permute-start.2 = (f16[128,4096]{1,0:T(8,128)(2,1)}, f16[128,4096]{1,0:T(8,128)(2,1)S(1)}, u32[]{:S(2)}, u32[]{:S(2)}) collective-permute-start(f16[128,4096]{1,0:T(8,128)(2,1)} %get-tuple-element.28), channel_id=1, source_target_pairs={{0,2},{2,0},{1,3},{3,1},{4,6},{6,4},{5,7},{7,5},{8,10},{10,8},{9,1... | collective-permute-start | bytes 3145736 | tf_op jit(solution)/shard_map/ppermute | solution.py:76
  94.5 38.9 %all-to-all-start = ((bf16[16,8,256]{2,1,0:T(8,128)(2,1)}), bf16[16,8,256]{2,1,0:T(8,128)(2,1)S(1)}, u32[]{:S(2)}, u32[]{:S(2)}) async-start(bf16[16,8,256]{2,1,0:T(8,128)(2,1)} %pad_maximum_fusion.6), calls=%async_computation | async-start | bytes 131072 | tf_op jit(solution)/shard_map/all_to_all | solution.py:170
  147.6 2.9 copy-start.7
  147.6 2.9 copy-start.14
  148.7 2.9 copy-start.3
  150.5 9.7 %collective-permute-start.3 = (f16[2,128,4096]{2,1,0:T(8,128)(2,1)}, f16[2,128,4096]{2,1,0:T(8,128)(2,1)}, u32[]{:S(2)}, u32[]{:S(2)}) collective-permute-start(f16[2,128,4096]{2,1,0:T(8,128)(2,1)} %pad_maximum_fusion), channel_id=1, source_target_pairs={{0,1},{1,0},{2,3},{3,2},{4,5},{5,4},{6,7},{7,6},{8,9},{9,8},{10,11... | collective-permute-start | bytes 6291464 | tf_op jit(solution)/shard_map/ppermute | solution.py:76
  153.2 2.0 copy-start.1
  153.2 2.2 copy-start.10
  159.5 4.5 %copy-start.5 = (bf16[8,2048]{1,0:T(8,128)(2,1)S(1)}, bf16[8,2048]{1,0:T(8,128)(2,1)}, u32[]{:S(2)}) copy-start(bf16[8,2048]{1,0:T(8,128)(2,1)} %param.24) | copy-start | bytes 98308
  159.9 5.4 %copy-start.8 = (f32[2048]{0:T(1024)S(1)}, f32[2048]{0:T(1024)}, u32[]{:S(2)}) copy-start(f32[2048]{0:T(1024)} %convert_element_type.262) | copy-start | bytes 24580
  159.9 5.5 %copy-start.6 = (f16[32,256]{1,0:T(8,128)(2,1)S(1)}, f16[32,256]{1,0:T(8,128)(2,1)}, u32[]{:S(2)}) copy-start(f16[32,256]{1,0:T(8,128)(2,1)} %convert_bitcast_fusion) | copy-start | bytes 49156
  162.7 7.7 %slice-start = ((f16[128,6272]{1,0:T(8,128)(2,1)}), f16[128,128]{1,0:T(8,128)(2,1)S(1)}, s32[]{:S(2)}) async-start(f16[128,6272]{1,0:T(8,128)(2,1)} %copy-done.2), calls=%async_computation.5 | async-start | bytes 65536 | tf_op jit(solution)/shard_map/slice | solution.py:157
  166.4 74.3 %all-to-all-start.1 = ((f16[8,32,1280]{2,1,0:T(8,128)(2,1)}), f16[8,32,1280]{2,1,0:T(8,128)(2,1)S(1)}, u32[]{:S(2)}, u32[]{:S(2)}) async-start(f16[8,32,1280]{2,1,0:T(8,128)(2,1)} %stack.41), calls=%async_computation.1 | async-start | bytes 1310720 | tf_op jit(solution)/shard_map/all_to_all | solution.py:238
  241.8 37.6 %all-to-all-start.2 = ((bf16[8,16,2048]{2,1,0:T(8,128)(2,1)}), bf16[8,16,2048]{2,1,0:T(8,128)(2,1)S(1)}, u32[]{:S(2)}, u32[]{:S(2)}) async-start(bf16[8,16,2048]{2,1,0:T(8,128)(2,1)} %bitcast.43), calls=%async_computation.2 | async-start | bytes 1048576 | tf_op jit(solution)/shard_map/all_to_all | solution.py:247
  250.9 28.6 %collective-permute-start.4 = (f16[256,768]{1,0:T(8,128)(2,1)S(1)}, f16[256,768]{1,0:T(8,128)(2,1)S(1)}, u32[]{:S(2)}, u32[]{:S(2)}) collective-permute-start(f16[256,768]{1,0:T(8,128)(2,1)S(1)} %get-tuple-element.32), channel_id=1, source_target_pairs={{0,4},{4,0},{1,5},{5,1},{2,6},{6,2},{3,7},{7,3},{8,12},{12,8},{9,1... | collective-permute-start | bytes 1179656 | tf_op jit(solution)/shard_map/ppermute | solution.py:76
  283.8 33.8 %all-to-all-start.3 = ((bf16[8,16,2048]{2,1,0:T(8,128)(2,1)}), bf16[8,16,2048]{2,1,0:T(8,128)(2,1)S(1)}, u32[]{:S(2)}, u32[]{:S(2)}) async-start(bf16[8,16,2048]{2,1,0:T(8,128)(2,1)} %bitcast.48), calls=%async_computation.3 | async-start | bytes 1048576 | tf_op jit(solution)/shard_map/all_to_all | solution.py:257
  291.8 25.8 %collective-permute-start.5 = (f16[2,256,768]{2,1,0:T(8,128)(2,1)S(1)}, f16[2,256,768]{2,1,0:T(8,128)(2,1)S(1)}, u32[]{:S(2)}, u32[]{:S(2)}) collective-permute-start(f16[2,256,768]{2,1,0:T(8,128)(2,1)S(1)} %get-tuple-element.30), channel_id=1, source_target_pairs={{0,2},{2,0},{1,3},{3,1},{4,6},{6,4},{5,7},{7,5},{8,10},{10,8},{9,1... | collective-permute-start | bytes 2359304 | tf_op jit(solution)/shard_map/ppermute | solution.py:76
  317.7 0.9 copy-start.4
  320.3 9.1 %collective-permute-start.6 = (f16[2,2,256,768]{3,2,1,0:T(8,128)(2,1)S(1)}, f16[2,2,256,768]{3,2,1,0:T(8,128)(2,1)}, u32[]{:S(2)}, u32[]{:S(2)}) collective-permute-start(f16[2,2,256,768]{3,2,1,0:T(8,128)(2,1)S(1)} %pad_maximum_fusion.1), channel_id=1, source_target_pairs={{0,1},{1,0},{2,3},{3,2},{4,5},{5,4},{6,7},{7,6},{8,9},{9,8},{10,11... | collective-permute-start | bytes 4718600 | tf_op jit(solution)/shard_map/ppermute | solution.py:76
  324.9 45.1 %all-to-all-start.4 = ((bf16[8,8,2048]{2,1,0:T(8,128)(2,1)}), bf16[8,8,2048]{2,1,0:T(8,128)(2,1)S(1)}, u32[]{:S(2)}, u32[]{:S(2)}) async-start(bf16[8,8,2048]{2,1,0:T(8,128)(2,1)} %fusion.1), calls=%async_computation.4 | async-start | bytes 524288 | tf_op jit(solution)/shard_map/all_to_all | solution.py:266
